TPU v7x, 512 devices: a whole 4x4x16 slice. The times are simulated.
512 devices in a mesh: ep: 32 (over z, core), tp: 16 (over y, x).
Axes of the slice: x: 4, y: 4, z: 16, core: 2. Of those that a mesh axis runs over, the one named last changes fastest.
Arguments:
- tokens: bfloat16 [512, 2048], P('ep'), may hold values from -6 to 6
- norm_gain: float32 [2048], replicated, may hold values from 0.1 to 1.9
- w_query: bfloat16 [2048, 2048], P('ep', 'tp'), may hold values from -0.125 to 0.125
- w_key: bfloat16 [2048, 2048], P('ep', 'tp'), may hold values from -0.125 to 0.125
- w_decay: bfloat16 [2048, 2048], P('ep', 'tp'), may hold values from -0.125 to 0.125
- w_value: bfloat16 [2048, 4096], P('ep', 'tp'), may hold values from -0.125 to 0.125
- w_outgate: bfloat16 [2048, 4096], P('ep', 'tp'), may hold values from -0.125 to 0.125
- decay_rate: float32 [2048], P('tp'), may hold values from 0.02 to 1
- state: float32 [512, 16, 128, 256], P('ep', 'tp'), may hold values from -15 to 15
- head_gain: float32 [256], replicated, may hold values from 0.1 to 1.9
- w_output: bfloat16 [4096, 2048], P('tp'), may hold values from -0.09375 to 0.09375
- moe_gain: float32 [2048], replicated, may hold values from 0.1 to 1.9
- expert_ids: int32 [512, 2], P('ep'), may hold values from 0 to 31, all different within a row; in each aligned block of 16 rows (0 to 15, 16 to 31, ...) at most 2 rows name the same one
- group_prob: float32 [512], P('ep'), may hold values from 0.3 to 1
- inner_prob: float32 [512, 2], P('ep'), may hold values from 0.05 to 1
- w_gate: bfloat16 [32, 2048, 2048], P('ep', None, 'tp'), may hold values from -0.125 to 0.125
- w_up: bfloat16 [32, 2048, 2048], P('ep', None, 'tp'), may hold values from -0.125 to 0.125
- w_down: bfloat16 [32, 2048, 2048], P('ep', 'tp'), may hold values from -0.125 to 0.125
Outputs:
- output: bfloat16 [512, 2048], P('ep', 'tp')
Inputs may be any that keep to these rules, and one draw needn't show every extreme that they name: `expert_ids`: the 2 experts of a token differ. In the rows of one index of ep no expert is named more than 2 times, a bound that some block reaches there.
All inputs are finite; a program needn't handle non-finite values.
Results may differ from a plain program's by a relative error of at most 0.025.
Values may be sent and summed in bfloat16 or wider, within the bound.
A program may use at most 64 MiB of HBM per device.

v0:
```python
import jax
import jax.numpy as jnp
from jax import lax
from jax.sharding import PartitionSpec as P

epsilon = 1e-05


def split_up(shard, dim, length):
    shape = shard.shape
    tiles = shard.reshape(*shape[:dim], length, shape[dim] // length, *shape[dim + 1 :])
    return jnp.moveaxis(tiles, dim, 0)


def summed_on_arrival(shard, axis, dim):
    tiles = split_up(shard, dim, lax.axis_size(axis))
    arrived = lax.all_to_all(tiles, axis, split_axis=0, concat_axis=0, tiled=True)
    return arrived.astype(jnp.float32).sum(axis=0)


def sent_together(arrays, axis, dim, along):
    both = jnp.concatenate(arrays, axis=along)
    filled, at, done = (lax.all_gather(both, axis, axis=dim, tiled=True), 0, [])
    for a in arrays:
        done.append(lax.slice_in_dim(filled, at, at + a.shape[along], axis=along))
        at += a.shape[along]
    return tuple(done)


def sent_to_all(shard, axis):
    length = lax.axis_size(axis)
    return lax.all_to_all(
        jnp.broadcast_to(shard[None], (length, *shard.shape)), axis, 0, 0, tiled=True
    )


def of_everyone(shard, axis):
    return sent_to_all(shard, axis).astype(jnp.float32).sum(axis=0)


def inverse_rms(values):
    return lax.rsqrt(jnp.mean(values * values, axis=-1, keepdims=True) + epsilon)


def slot_numbers(route_ids, experts, capacity):
    flat_ids = route_ids.reshape(-1)
    onehot = (flat_ids[:, None] == jnp.arange(experts, dtype=jnp.int32)[None, :]).astype(jnp.int32)
    earlier = jnp.cumsum(onehot, axis=0) - onehot
    within = jnp.sum(earlier * onehot, axis=1)
    return (flat_ids * capacity + within).reshape(route_ids.shape)


def expert_apply(rows, weight_gate, weight_up, weight_down):
    gate = jnp.dot(rows, weight_gate, preferred_element_type=jnp.float32)
    upper = jnp.dot(rows, weight_up, preferred_element_type=jnp.float32)
    hidden = (jax.nn.silu(gate) * upper).astype(jnp.bfloat16)
    block_out = jnp.dot(hidden, weight_down, preferred_element_type=jnp.float32).astype(
        jnp.bfloat16
    )
    summed = summed_on_arrival(block_out.astype(jnp.float32).astype(jnp.bfloat16), "tp", 1)
    return summed.astype(jnp.bfloat16)


def on_device(
    tokens,
    norm_gain,
    w_query,
    w_key,
    w_decay,
    w_value,
    w_outgate,
    decay_rate,
    state,
    head_gain,
    w_output,
    moe_gain,
    expert_ids,
    group_prob,
    inner_prob,
    w_gate,
    w_up,
    w_down,
):
    wide = jnp.float32
    narrow = jnp.bfloat16
    seq_count = tokens.shape[0]
    model_width = tokens.shape[1]
    ep_count = lax.axis_size("ep")
    heads = state.shape[1]
    key_width = state.shape[2]
    value_width = state.shape[3]
    residual = tokens.astype(wide)
    normed = (residual * inverse_rms(residual) * norm_gain).astype(narrow)
    pieces = sent_together((w_query, w_key, w_decay, w_value, w_outgate), "ep", 0, 1)
    projected = jnp.concatenate(
        [jnp.dot(normed, piece, preferred_element_type=wide) for piece in pieces], axis=1
    )
    query_cols = w_query.shape[1]
    value_cols = w_value.shape[1]
    query = projected[:, :query_cols].astype(narrow).astype(wide).reshape(
        seq_count, heads, key_width
    ) * key_width ** (-0.5)
    key_rows = (
        projected[:, query_cols : 2 * query_cols]
        .astype(narrow)
        .astype(wide)
        .reshape(seq_count, heads, key_width)
    )
    decay_pre = projected[:, 2 * query_cols : 3 * query_cols]
    value_rows = (
        projected[:, 3 * query_cols : 3 * query_cols + value_cols].astype(narrow).astype(wide)
    )
    value_rows = value_rows.reshape(seq_count, heads, value_width)
    gate_rows = (
        projected[:, 3 * query_cols + value_cols :]
        .astype(narrow)
        .astype(wide)
        .reshape(seq_count, heads, value_width)
    )
    decay = jnp.exp(jax.nn.log_sigmoid(decay_pre) * decay_rate).reshape(seq_count, heads, key_width)
    updated = decay[..., None] * state + key_rows[..., None] * value_rows[:, :, None, :]
    readout = jnp.einsum("shk,shkv->shv", query, updated)
    gated = (readout * inverse_rms(readout) * head_gain * jax.nn.silu(gate_rows)).astype(narrow)
    head_part = jnp.dot(
        gated.reshape(seq_count, heads * value_width), w_output, preferred_element_type=wide
    )
    attention = of_everyone(
        head_part.astype(narrow).astype(wide).astype(jnp.bfloat16), "tp"
    ).astype(jnp.float32)
    mixed_wide = (residual + attention).astype(narrow).astype(wide)
    moe_in = (mixed_wide * inverse_rms(mixed_wide) * moe_gain).astype(narrow)
    route_weight = group_prob[:, None] * inner_prob / jnp.sum(inner_prob, axis=1, keepdims=True)
    top = expert_ids.shape[1]
    capacity = 2 * seq_count * top // ep_count
    slot_total = ep_count * capacity
    col_width = model_width // lax.axis_size("tp")
    col_start = lax.axis_index("tp") * col_width
    slots = slot_numbers(expert_ids, ep_count, capacity)
    slot_range = jnp.arange(slot_total, dtype=jnp.int32)
    combine = jnp.sum(
        jnp.where(slots[:, :, None] == slot_range[None, None, :], route_weight[:, :, None], 0.0),
        axis=1,
    )
    dispatch = jnp.any(slots[None, :, :] == slot_range[:, None, None], axis=2).astype(narrow)
    sending = jnp.dot(dispatch, moe_in, preferred_element_type=wide).astype(narrow)
    arrived = lax.all_to_all(sending, "ep", split_axis=0, concat_axis=0, tiled=True)
    expert_out = expert_apply(arrived, w_gate[0], w_up[0], w_down[0])
    returned = lax.all_to_all(expert_out, "ep", split_axis=0, concat_axis=0, tiled=True).astype(
        wide
    )
    moe_sum = jnp.dot(combine, returned)
    own_cols = lax.dynamic_slice_in_dim(mixed_wide, col_start, col_width, 1)
    return (own_cols + moe_sum).astype(narrow)


def solution(mesh):
    placed = (
        P("ep", None),
        P(),
        P("ep", "tp"),
        P("ep", "tp"),
        P("ep", "tp"),
        P("ep", "tp"),
        P("ep", "tp"),
        P("tp"),
        P("ep", "tp", None, None),
        P(),
        P("tp", None),
        P(),
        P("ep", None),
        P("ep"),
        P("ep", None),
        P("ep", None, "tp"),
        P("ep", None, "tp"),
        P("ep", "tp", None),
    )
    return jax.shard_map(
        on_device, mesh=mesh, in_specs=placed, out_specs=P("ep", "tp"), check_vma=False
    )
```

profile of v0, /device:TPU:1, one launch (start us, length us, event | category | flops | bytes accessed | tf_op | source)
XLA Modules:
  0.0 194.8 jit_solution(7613276063330362409)
XLA Ops:
  6.5 0.0 copy-start
  6.5 0.0 copy-start.2
  6.5 0.0 copy-start.6
  6.5 0.0 copy-start.1
  6.5 0.0 copy-start.10
  6.5 0.0 all-gather.2.cloned.1.call-start
  6.6 0.9 constant_dynamic-update-slice_fusion.4
  7.5 0.8 constant_dynamic-update-slice_fusion.3
  8.3 0.7 constant_dynamic-update-slice_fusion.2
  9.0 0.8 constant_dynamic-update-slice_fusion.1
  9.7 0.8 constant_dynamic-update-slice_fusion
  10.5 0.0 copy-start.5
  10.5 0.6 copy-done.5
  11.1 0.0 all-gather.2.cloned.1.call-update
  11.2 1.0 fusion.26
  12.1 77.9 %all-gather.2.cloned.1.call-done = bf16[2048,896]{1,0:T(8,128)(2,1)} async-done(((bf16[64,896]{1,0:T(8,128)(2,1)}), bf16[2048,896]{1,0:T(8,128)(2,1)}) %all-gather.2.cloned.1.call-update) | async-done | bytes 3670032 | tf_op jit(solution)/shard_map/all_gather | solution.py:23
  90.0 1.6 fusion.8
  91.6 1.3 fusion.12
  92.9 1.3 fusion.10
  94.2 1.4 fusion.52
  95.6 0.0 copy-done.1
  95.6 0.0 copy-start.8
  95.6 0.9 fusion
  96.6 0.1 fusion.38
  96.7 0.0 copy-done
  96.7 0.0 copy-done.2
  96.7 0.0 copy-done.6
  96.7 0.0 copy-done.10
  96.7 2.0 %convolution_convert_fusion.2 = bf16[16,2048]{1,0:T(8,128)(2,1)S(1)} fusion(bf16[256,2048]{1,0:T(8,128)(2,1)S(1)} %copy-done, bf16[2048,896]{1,0:T(8,128)(2,1)} %all-gather.2.cloned.1.call-done, f32[16,1,256]{2,1,0:T(1,128)S(1)} %fusion, f32[256]{0:T(256)S(1)} %copy-done.10, f32[16]{0:T(128)S(1)} %add_rsqrt_fusion.1, bf16[16,2048]{1,0:T(8,128)(2,1)S(1)} %copy-done.2, ...), kind=kOutput, calls=%fused_computation.2 | convolution fusion | flops 33759232 | bytes 2253952 | tf_op jit(solution)/shard_map/dot_general | solution.py:124
  98.7 1.1 broadcast_in_dim.10
  99.9 6.5 %all-to-all-start = ((bf16[16,16,2048]{2,1,0:T(8,128)(2,1)}), bf16[16,16,2048]{2,1,0:T(8,128)(2,1)S(1)}, u32[]{:S(2)}, u32[]{:S(2)}) async-start(bf16[16,16,2048]{2,1,0:T(8,128)(2,1)} %broadcast_in_dim.10), calls=%async_computation | async-start | bytes 2097152 | tf_op jit(solution)/shard_map/all_to_all | solution.py:32
  106.4 0.0 copy-done.8
  106.4 0.0 copy-start.9
  106.4 0.0 copy-start.11
  106.4 0.1 copy.38
  106.5 0.1 eq.20
  106.6 0.1 fusion.43
  106.7 0.1 reduce_window_sum.11
  106.7 0.2 select_reduce_fusion.1
  106.9 0.1 reduce_sum.81
  107.0 0.1 copy.39
  107.1 0.1 fusion.48
  107.2 15.7 %all-to-all-done = bf16[16,16,2048]{2,1,0:T(8,128)(2,1)S(1)} async-done(((bf16[16,16,2048]{2,1,0:T(8,128)(2,1)}), bf16[16,16,2048]{2,1,0:T(8,128)(2,1)S(1)}, u32[]{:S(2)}, u32[]{:S(2)}) %all-to-all-start) | async-done | bytes 1048608 | tf_op jit(solution)/shard_map/all_to_all | solution.py:32
  122.8 0.1 convert_reduce_fusion
  123.0 0.1 multiply_reduce_fusion
  123.1 0.0 copy-done.7
  123.1 0.3 convolution_convert_fusion.1
  123.4 0.2 all_to_all.23
  123.6 31.8 %all_to_all.34 = bf16[32,2,2048]{2,1,0:T(2,128)(2,1)S(1)} all-to-all(bf16[32,2,2048]{2,1,0:T(2,128)(2,1)S(1)} %all_to_all.23), channel_id=1, replica_groups=mesh['ep'=32,'tp'=16] {'ep'}, dimensions={0} | all-to-all | bytes 524288 | tf_op jit(solution)/shard_map/all_to_all | solution.py:146
  155.4 0.1 all_to_all.25
  155.5 1.3 fusion.24
  156.8 0.0 copy-done.3
  156.8 0.0 copy-done.4
  156.8 0.4 fusion.5
  157.2 0.8 copy.50
  158.0 3.5 %all-to-all-start.2 = ((bf16[16,64,128]{2,1,0:T(8,128)(2,1)}), bf16[16,64,128]{2,1,0:T(8,128)(2,1)S(1)}, u32[]{:S(2)}, u32[]{:S(2)}) async-start(bf16[16,64,128]{2,1,0:T(8,128)(2,1)} %bitcast.45), calls=%async_computation.2 | async-start | bytes 524288 | tf_op jit(solution)/shard_map/all_to_all | solution.py:17
  161.5 0.0 copy-done.9
  161.6 0.0 copy-done.11
  161.6 8.0 %all-to-all-done.2 = bf16[16,64,128]{2,1,0:T(8,128)(2,1)S(1)} async-done(((bf16[16,64,128]{2,1,0:T(8,128)(2,1)}), bf16[16,64,128]{2,1,0:T(8,128)(2,1)S(1)}, u32[]{:S(2)}, u32[]{:S(2)}) %all-to-all-start.2) | async-done | bytes 262176 | tf_op jit(solution)/shard_map/all_to_all | solution.py:17
  169.6 0.6 reduce_sum.85
  170.2 5.0 %all-to-all-start.3 = ((bf16[32,2,128]{2,1,0:T(2,128)(2,1)}), bf16[32,2,128]{2,1,0:T(2,128)(2,1)S(1)}, u32[]{:S(2)}, u32[]{:S(2)}) async-start(bf16[32,2,128]{2,1,0:T(2,128)(2,1)} %bitcast.8), calls=%async_computation.3 | async-start | bytes 32768 | tf_op jit(solution)/shard_map/all_to_all | solution.py:148
  175.3 0.1 select_reduce_fusion
  175.4 11.8 %all-to-all-done.3 = bf16[32,2,128]{2,1,0:T(2,128)(2,1)S(1)} async-done(((bf16[32,2,128]{2,1,0:T(2,128)(2,1)}), bf16[32,2,128]{2,1,0:T(2,128)(2,1)S(1)}, u32[]{:S(2)}, u32[]{:S(2)}) %all-to-all-start.3) | async-done | bytes 16416 | tf_op jit(solution)/shard_map/all_to_all | solution.py:148
  187.2 0.7 fusion.9
  (9 shorter events, 0.1 us)
Async XLA Ops:
  6.5 90.2 %copy-start = (bf16[256,2048]{1,0:T(8,128)(2,1)S(1)}, bf16[256,2048]{1,0:T(8,128)(2,1)}, u32[]{:S(2)}) copy-start(bf16[256,2048]{1,0:T(8,128)(2,1)} %param.28) | copy-start | bytes 3145732
  6.5 90.2 %copy-start.2 = (bf16[16,2048]{1,0:T(8,128)(2,1)S(1)}, bf16[16,2048]{1,0:T(8,128)(2,1)}, u32[]{:S(2)}) copy-start(bf16[16,2048]{1,0:T(8,128)(2,1)} %param.18) | copy-start | bytes 196612
  6.5 90.2 %copy-start.6 = (f32[2048]{0:T(1024)S(1)}, f32[2048]{0:T(1024)}, u32[]{:S(2)}) copy-start(f32[2048]{0:T(1024)} %param.19) | copy-start | bytes 24580
  6.5 89.1 %copy-start.1 = (f32[16,1,128,256]{3,2,1,0:T(8,128)S(1)}, f32[16,1,128,256]{3,2,1,0:T(8,128)}, u32[]{:S(2)}) copy-start(f32[16,1,128,256]{3,2,1,0:T(8,128)} %param.26) | copy-start | bytes 6291460
  6.5 90.2 %copy-start.10 = (f32[256]{0:T(256)S(1)}, f32[256]{0:T(256)}, u32[]{:S(2)}) copy-start(f32[256]{0:T(256)} %param.27) | copy-start | bytes 3076
  6.5 83.5 %all-gather.2.cloned.1.call-start = ((), (), s32[]{:S(2)}) async-start(), calls=%async_computation.4 | async-start | bytes 3784704 | tf_op jit(solution)/shard_map/all_gather | solution.py:23
  10.5 0.6 copy-start.5
  95.6 10.8 %copy-start.8 = (s32[16,2]{0,1:T(2,128)S(1)}, s32[16,2]{0,1:T(2,128)}, u32[]{:S(2)}) copy-start(s32[16,2]{0,1:T(2,128)} %param.30) | copy-start | bytes 388
  96.6 26.6 %copy-start.7 = (f32[2048]{0:T(1024)S(1)}, f32[2048]{0:T(1024)}, u32[]{:S(2)}) copy-start(f32[2048]{0:T(1024)} %param.29) | copy-start | bytes 24580
  98.7 58.1 %copy-start.3 = (bf16[1,128,2048]{2,1,0:T(8,128)(2,1)S(1)}, bf16[1,128,2048]{2,1,0:T(8,128)(2,1)}, u32[]{:S(2)}) copy-start(bf16[1,128,2048]{2,1,0:T(8,128)(2,1)} %param.35) | copy-start | bytes 1572868
  98.7 58.1 %copy-start.4 = (bf16[1,2048,128]{2,1,0:T(8,128)(2,1)S(1)}, bf16[1,2048,128]{2,1,0:T(8,128)(2,1)}, u32[]{:S(2)}) copy-start(bf16[1,2048,128]{2,1,0:T(8,128)(2,1)} %param.34) | copy-start | bytes 1572868
  99.9 23.0 %all-to-all-start = ((bf16[16,16,2048]{2,1,0:T(8,128)(2,1)}), bf16[16,16,2048]{2,1,0:T(8,128)(2,1)S(1)}, u32[]{:S(2)}, u32[]{:S(2)}) async-start(bf16[16,16,2048]{2,1,0:T(8,128)(2,1)} %broadcast_in_dim.10), calls=%async_computation | async-start | bytes 2097152 | tf_op jit(solution)/shard_map/all_to_all | solution.py:32
  106.4 55.1 %copy-start.9 = (f32[16,2]{0,1:T(2,128)S(1)}, f32[16,2]{0,1:T(2,128)}, u32[]{:S(2)}) copy-start(f32[16,2]{0,1:T(2,128)} %param.32) | copy-start | bytes 388
  106.4 55.1 %copy-start.11 = (f32[16]{0:T(128)S(1)}, f32[16]{0:T(128)}, u32[]{:S(2)}) copy-start(f32[16]{0:T(128)} %param.31) | copy-start | bytes 196
  158.0 11.6 %all-to-all-start.2 = ((bf16[16,64,128]{2,1,0:T(8,128)(2,1)}), bf16[16,64,128]{2,1,0:T(8,128)(2,1)S(1)}, u32[]{:S(2)}, u32[]{:S(2)}) async-start(bf16[16,64,128]{2,1,0:T(8,128)(2,1)} %bitcast.45), calls=%async_computation.2 | async-start | bytes 524288 | tf_op jit(solution)/shard_map/all_to_all | solution.py:17
  170.2 16.9 %all-to-all-start.3 = ((bf16[32,2,128]{2,1,0:T(2,128)(2,1)}), bf16[32,2,128]{2,1,0:T(2,128)(2,1)S(1)}, u32[]{:S(2)}, u32[]{:S(2)}) async-start(bf16[32,2,128]{2,1,0:T(2,128)(2,1)} %bitcast.8), calls=%async_computation.3 | async-start | bytes 32768 | tf_op jit(solution)/shard_map/all_to_all | solution.py:148
Sparse Core Ops, SparseCore 0:
  11.3 78.6 all-gather.1
where the time goes:
time: 195 us
  waiting for transfers between devices  113 us (58%)
  blocking collectives  31.8 us (16%)
  starting transfers between devices  15.1 us (8%)
  between operations  13.6 us (7%)
  matrix products  11.2 us (6%)
  local copies, waits for them, and re-layouts  7.11 us (4%)
  other arithmetic  2.53 us (1%)
    all_gather x1, waiting for transfers between devices, sent_together(): filled, at, done = (lax.all_gather(both, axis, axis=dim, tiled=True), 0, [])  77.9 us
    all_to_all x1, blocking collectives, on_device(): lax.all_to_all(sending, 'ep', split_axis=0, concat_axis=0, tiled=True)  31.8 us
    all_to_all x1, waiting for transfers between devices, sent_to_all(): lax.all_to_all(jnp.broadcast_to(shard[None], (length, *shard.shape)), axi...  15.7 us
    all_to_all x1, waiting for transfers between devices, on_device(): lax.all_to_all(expert_out, 'ep', split_axis=0, concat_axis=0, tiled=True)  11.8 us
    all_to_all x1, waiting for transfers between devices, summed_on_arrival(): lax.all_to_all(tiles, axis, split_axis=0, concat_axis=0, tiled=True)  8.02 us
    all_to_all x1, starting transfers between devices, sent_to_all(): lax.all_to_all(jnp.broadcast_to(shard[None], (length, *shard.shape)), axi...  6.53 us
    dot_general x4, matrix products, on_device(): jnp.dot(normed, piece, preferred_element_type=wide)  5.61 us
    all_to_all x1, starting transfers between devices, on_device(): lax.all_to_all(expert_out, 'ep', split_axis=0, concat_axis=0, tiled=True)  5.03 us
  transfers between devices with their start and end apart: 4, of which 4 were waited for; matrix products, arithmetic and copies ran while one was open for 1% of the time, Pallas kernels for 0%

commit v1 on v0

v1 whole, which is shorter than its diff:
```python
import functools

import jax
import jax.numpy as jnp
from jax import lax
from jax.experimental import pallas as pl
from jax.experimental.pallas import tpu as pltpu
from jax.sharding import PartitionSpec as P

epsilon = 1e-05
MESH = pl.DeviceIdType.MESH
wide = jnp.float32
narrow = jnp.bfloat16


def kernel(
    E,
    T,
    tokens,
    norm_gain,
    w_query,
    w_key,
    w_decay,
    w_value,
    w_outgate,
    decay_rate,
    state,
    head_gain,
    w_output,
    moe_gain,
    expert_ids,
    group_prob,
    inner_prob,
    w_gate,
    w_up,
    w_down,
    out,
    wall,
    nbuf,
    acc,
    st_v,
    wo_v,
    wgu_v,
    wdn_v,
    head_send,
    head_recv,
    disp_send,
    disp_recv,
    rows_all,
    down_send,
    down_recv,
    ret_send,
    ret_recv,
    mixed_v,
    w_sem,
    big_sem,
    ring_send,
    d2d_send,
    ring_recv,
    d2d_recv,
    phase_send,
    phase_recv,
    rows_recv,
):
    Z = E // 2
    half = Z // 2
    S, D = tokens.shape
    KB = w_query.shape[0]
    CW = D // T
    QC = w_query.shape[1]
    VC = w_value.shape[1]
    FB = w_down.shape[0]
    DK = state.shape[1]
    e = lax.axis_index("ep")
    h = lax.axis_index("tp")
    z = e // 2
    c = e % 2
    own_rows = pl.ds(pl.multiple_of(c * KB, KB), KB)
    peer_rows = pl.ds(pl.multiple_of((1 - c) * KB, KB), KB)

    parts = (
        (w_query, 0, QC),
        (w_key, QC, QC),
        (w_value, 2 * QC, VC),
        (w_outgate, 2 * QC + VC, VC),
        (w_decay, 2 * QC + 2 * VC, QC),
    )
    loads = []
    for i, (ref, at, width) in enumerate(parts):
        loads.append(
            pltpu.make_async_copy(ref, wall.at[z, own_rows, pl.ds(at, width)], w_sem.at[i])
        )
        loads[-1].start()
    big = [
        pltpu.make_async_copy(state, st_v, big_sem.at[0]),
        pltpu.make_async_copy(w_output, wo_v, big_sem.at[1]),
        pltpu.make_async_copy(w_gate, wgu_v.at[:, pl.ds(0, FB)], big_sem.at[2]),
        pltpu.make_async_copy(w_up, wgu_v.at[:, pl.ds(FB, FB)], big_sem.at[3]),
        pltpu.make_async_copy(w_down, wdn_v, big_sem.at[4]),
    ]

    up_dev = (2 * ((z + 1) % Z) + c, h)
    down_dev = (2 * ((z + Z - 1) % Z) + c, h)
    peer = (2 * z + 1 - c, h)
    barrier = pltpu.get_barrier_semaphore()
    for dev in (up_dev, down_dev, peer):
        pl.semaphore_signal(barrier, inc=1, device_id=dev, device_id_type=MESH)

    def greet(i, _):
        pl.semaphore_signal(
            barrier, inc=1, device_id=(e, (h + i) % T), device_id_type=MESH
        )
        return 0

    lax.fori_loop(1, T, greet, 0)
    for copy in big:
        copy.start()

    residual = tokens[...].astype(wide)
    scale = lax.rsqrt(jnp.mean(residual * residual, axis=-1, keepdims=True) + epsilon)
    normed = (residual * scale * norm_gain[...]).astype(narrow)
    for i in range(Z):
        nbuf[i] = normed[:, 2 * KB * i : 2 * KB * (i + 1)]
    pl.semaphore_wait(barrier, 3 + T - 1)

    chunks = (
        (0, 2 * QC, (0, 1)),
        (2 * QC, VC, (2,)),
        (2 * QC + VC, VC, (3,)),
        (2 * QC + 2 * VC, QC, (4,)),
    )
    whole = range(len(chunks))
    dirs = ((up_dev, -1, (0, 1)), (down_dev, 1, (2, 3)))

    def block(zz, rows, ch):
        return wall.at[zz, rows, pl.ds(chunks[ch][0], chunks[ch][1])]

    def ring_copy(d, zz, s, ch):
        return pltpu.make_async_remote_copy(
            src_ref=block(zz, own_rows, ch),
            dst_ref=block(zz, own_rows, ch),
            send_sem=ring_send.at[d, s, ch],
            recv_sem=ring_recv.at[d, s, ch],
            device_id=dirs[d][0],
            device_id_type=MESH,
        )

    def peer_copy(d, zz, s, ch, rows):
        return pltpu.make_async_remote_copy(
            src_ref=block(zz, rows, ch),
            dst_ref=block(zz, rows, ch),
            send_sem=d2d_send.at[d, s, ch],
            recv_sem=d2d_recv.at[d, s, ch],
            device_id=peer,
            device_id_type=MESH,
        )

    def at_step(d, s):
        return (z + dirs[d][1] * s + 2 * Z) % Z

    def multiply(zz, ch):
        cols = slice(chunks[ch][0], chunks[ch][0] + chunks[ch][1])
        acc[:, cols] += jnp.dot(nbuf[zz], wall[zz, :, cols], preferred_element_type=wide)

    acc[...] = jnp.zeros_like(acc)
    for ch in whole:
        for i in chunks[ch][2]:
            loads[i].wait()
        for d in (0, 1):
            if half > 1 or ch in dirs[d][2]:
                ring_copy(d, z, 1, ch).start()
        peer_copy(0, z, 0, ch, own_rows).start()

    def step_of(s, first, before_last, last):
        for ch in whole:
            for d in (0, 1):
                if last and ch not in dirs[d][2]:
                    continue
                zz = at_step(d, s)
                ring_copy(d, zz, s, ch).wait_recv()
                if not last and (not before_last or ch in dirs[d][2]):
                    ring_copy(d, zz, s + 1, ch).start()
                peer_copy(d, zz, s, ch, own_rows).start()
            for d in (0,) if first else (0, 1):
                zz = at_step(d, s - 1)
                peer_copy(d, zz, s - 1, ch, peer_rows).wait_recv()
                multiply(zz, ch)

    if half > 1:
        step_of(1, True, half == 2, False)

        def middle(s, _):
            step_of(s, False, False, False)
            return 0

        if half > 3:
            lax.fori_loop(2, half - 1, middle, 0)
        elif half == 3:
            pass
        if half > 2:
            step_of(half - 1, False, True, False)
    step_of(half, half == 1, False, True)
    for d in (0, 1):
        for ch in dirs[d][2]:
            zz = at_step(d, half)
            peer_copy(d, zz, half, ch, peer_rows).wait_recv()
            multiply(zz, ch)

    def rounded(at, width):
        return acc[:, at : at + width].astype(narrow).astype(wide)

    query = rounded(0, QC) * DK ** (-0.5)
    key_rows = rounded(QC, QC)
    value_rows = rounded(2 * QC, VC)
    gate_rows = rounded(2 * QC + VC, VC)
    decay_pre = acc[:, 2 * QC + 2 * VC :]
    decay = jnp.exp(
        (jnp.minimum(decay_pre, 0.0) - jnp.log1p(jnp.exp(-jnp.abs(decay_pre)))) * decay_rate[...]
    )
    fresh = jnp.sum(query * key_rows, axis=1, keepdims=True) * value_rows
    turned = jnp.transpose(query * decay)
    big[0].wait()
    read = [
        jnp.sum(turned[:, i : i + 1] * st_v[i], axis=0, keepdims=True) for i in range(S)
    ]
    readout = jnp.concatenate(read, axis=0) + fresh
    size = lax.rsqrt(jnp.mean(readout * readout, axis=-1, keepdims=True) + epsilon)
    gated = (readout * size * head_gain[...] * jax.nn.silu(gate_rows)).astype(narrow)

    def whole_wait(ref, count, sem):
        pltpu.make_async_copy(ref.at[pl.ds(0, count)], ref.at[pl.ds(0, count)], sem).wait()

    def to_plane(src, dst, phase):
        def send(i, _):
            to = (h + i) % T
            pltpu.make_async_remote_copy(
                src_ref=src.at[to],
                dst_ref=dst.at[h],
                send_sem=phase_send.at[phase],
                recv_sem=phase_recv.at[phase],
                device_id=(e, to),
                device_id_type=MESH,
            ).start()
            return 0

        lax.fori_loop(1, T, send, 0)

    def to_column(src, dst, phase):
        def send(i, _):
            to = (e + i) % E
            pltpu.make_async_remote_copy(
                src_ref=src.at[to],
                dst_ref=dst.at[e],
                send_sem=phase_send.at[phase],
                recv_sem=phase_recv.at[phase],
                device_id=(to, h),
                device_id_type=MESH,
            ).start()
            return 0

        lax.fori_loop(1, E, send, 0)

    def in_slices(left, right_ref, dst):
        step = 2 if T % 2 == 0 else 1
        for i in range(0, T, step):
            both = jnp.dot(
                left, right_ref[:, i * CW : (i + step) * CW], preferred_element_type=wide
            ).astype(narrow)
            for j in range(step):
                dst[i + j] = both[:, j * CW : (j + 1) * CW]

    big[1].wait()
    in_slices(gated, wo_v, head_send)
    to_plane(head_send, head_recv, 0)
    head_recv[h] = head_send[h]

    ids = expert_ids[...]
    experts = lax.broadcasted_iota(jnp.int32, (S, E), 1)
    chosen = [ids[:, k : k + 1] == experts for k in range(ids.shape[1])]
    named = functools.reduce(jnp.logical_or, chosen)
    marks = jnp.where(named, 1.0, 0.0).astype(narrow)
    later = lax.broadcasted_iota(jnp.int32, (S, S), 0) > lax.broadcasted_iota(jnp.int32, (S, S), 1)
    rank = jnp.dot(
        jnp.where(later, 1.0, 0.0).astype(narrow), marks, preferred_element_type=wide
    ).astype(jnp.int32)
    inner = inner_prob[...]
    route = group_prob[...] * inner / jnp.sum(inner, axis=1, keepdims=True)
    weight = sum(jnp.where(m, route[:, k : k + 1], 0.0) for k, m in enumerate(chosen))
    per_slot = disp_send.shape[1]
    picked = [jnp.where(named & (rank == r), 1.0, 0.0) for r in range(per_slot)]
    picked_rows = [jnp.transpose(p).astype(narrow) for p in picked]

    whole_wait(head_recv, T - 1, phase_recv.at[0])
    attention = functools.reduce(jnp.add, [head_recv[i].astype(wide) for i in range(T)])
    own_cols = pl.ds(pl.multiple_of(h * CW, CW), CW)
    mixed = (tokens[:, own_cols].astype(wide) + attention).astype(narrow)
    mixed_v[...] = mixed.astype(wide)

    for r in range(per_slot):
        disp_send[:, r, :] = jnp.dot(picked_rows[r], mixed, preferred_element_type=wide)
    to_column(disp_send, disp_recv, 1)
    disp_recv[e] = disp_send[e]
    whole_wait(head_send, T - 1, phase_send.at[0])
    for i in (2, 3, 4):
        big[i].wait()
    whole_wait(disp_recv, E - 1, phase_recv.at[1])

    for r in range(per_slot):
        rows_all[h, r * E : (r + 1) * E, :] = disp_recv[:, r, :].astype(narrow)

    def rows_copy(i, to):
        return pltpu.make_async_remote_copy(
            src_ref=rows_all.at[i],
            dst_ref=rows_all.at[i],
            send_sem=phase_send.at[2],
            recv_sem=rows_recv.at[i],
            device_id=(e, to),
            device_id_type=MESH,
        )

    def spread(i, _):
        rows_copy(h, (h + i) % T).start()
        return 0

    lax.fori_loop(1, T, spread, 0)

    def gate_up(i, carry):
        total, squares = carry
        at = pl.multiple_of(i * CW, CW)
        x = rows_all[i].astype(wide)
        scaled = (x * moe_gain[:, pl.ds(at, CW)]).astype(narrow)
        total += jnp.dot(scaled, wgu_v[pl.ds(at, CW), :], preferred_element_type=wide)
        return total, squares + jnp.sum(x * x, axis=1, keepdims=True)

    rows_n = E * per_slot
    carry = gate_up(h, (jnp.zeros((rows_n, 2 * FB), wide), jnp.zeros((rows_n, 1), wide)))

    def next_cols(i, carry):
        at = (h + T - i) % T
        rows_copy(at, h).wait_recv()
        return gate_up(at, carry)

    total, squares = lax.fori_loop(1, T, next_cols, carry)
    total = total * lax.rsqrt(squares / D + epsilon)
    hidden = (jax.nn.silu(total[:, :FB]) * total[:, FB:]).astype(narrow)

    in_slices(hidden, wdn_v, down_send)
    to_plane(down_send, down_recv, 3)
    down_recv[h] = down_send[h]
    whole_wait(disp_send, E - 1, phase_send.at[1])
    whole_wait(rows_all, T - 1, phase_send.at[2])
    whole_wait(down_recv, T - 1, phase_recv.at[3])
    expert_out = functools.reduce(jnp.add, [down_recv[i].astype(wide) for i in range(T)])
    expert_out = expert_out.astype(narrow).astype(wide)

    for r in range(per_slot):
        ret_send[:, r, :] = expert_out[r * E : (r + 1) * E]
    to_column(ret_send, ret_recv, 4)
    ret_recv[e] = ret_send[e]
    whole_wait(down_send, T - 1, phase_send.at[3])
    for ch in whole:
        peer_copy(0, z, 0, ch, own_rows).wait_send()
        for d in (0, 1):
            for s in range(1, half):
                ring_copy(d, z, s, ch).wait_send()
                peer_copy(d, z, s, ch, own_rows).wait_send()
            if ch in dirs[d][2]:
                ring_copy(d, z, half, ch).wait_send()
                peer_copy(d, z, half, ch, own_rows).wait_send()
    whole_wait(ret_recv, E - 1, phase_recv.at[4])
    result = mixed_v[...]
    for r in range(per_slot):
        result += jnp.dot(
            picked[r] * weight,
            ret_recv[:, r, :],
            preferred_element_type=wide,
            precision=lax.Precision.HIGHEST,
        )
    out[...] = result.astype(narrow)
    whole_wait(ret_send, E - 1, phase_send.at[4])


def on_device(E, T, *args):
    (
        tokens,
        norm_gain,
        w_query,
        w_key,
        w_decay,
        w_value,
        w_outgate,
        decay_rate,
        state,
        head_gain,
        w_output,
        moe_gain,
        expert_ids,
        group_prob,
        inner_prob,
        w_gate,
        w_up,
        w_down,
    ) = args
    S, D = tokens.shape
    KB, QC = w_query.shape
    VC = w_value.shape[1]
    FB = w_down.shape[1]
    CW = D // T
    Z = E // 2
    steps = Z // 2 + 1
    slots = max(2, S * expert_ids.shape[1] // E)
    vmem = pl.BlockSpec(memory_space=pltpu.VMEM)
    hbm = pl.BlockSpec(memory_space=pl.ANY)
    cols = 3 * QC + 2 * VC
    dma = pltpu.SemaphoreType.DMA
    return pl.pallas_call(
        functools.partial(kernel, E, T),
        out_shape=jax.ShapeDtypeStruct((S, CW), narrow),
        in_specs=[vmem, vmem, hbm, hbm, hbm, hbm, hbm, vmem, hbm, vmem, hbm]
        + [vmem, vmem, vmem, vmem, hbm, hbm, hbm],
        out_specs=vmem,
        scratch_shapes=[
            pltpu.VMEM((Z, 2 * KB, cols), narrow),
            pltpu.VMEM((Z, S, 2 * KB), narrow),
            pltpu.VMEM((S, cols), wide),
            pltpu.VMEM((S, QC, VC), wide),
            pltpu.VMEM((VC, D), narrow),
            pltpu.VMEM((D, 2 * FB), narrow),
            pltpu.VMEM((FB, D), narrow),
            pltpu.VMEM((T, S, CW), narrow),
            pltpu.VMEM((T, S, CW), narrow),
            pltpu.VMEM((E, slots, CW), wide),
            pltpu.VMEM((E, slots, CW), wide),
            pltpu.VMEM((T, E * slots, CW), narrow),
            pltpu.VMEM((T, E * slots, CW), narrow),
            pltpu.VMEM((T, E * slots, CW), narrow),
            pltpu.VMEM((E, slots, CW), wide),
            pltpu.VMEM((E, slots, CW), wide),
            pltpu.VMEM((S, CW), wide),
            dma((5,)),
            dma((5,)),
            dma((2, steps, 4)),
            dma((2, steps, 4)),
            dma((2, steps, 4)),
            dma((2, steps, 4)),
            dma((5,)),
            dma((5,)),
            dma((T,)),
        ],
        compiler_params=pltpu.CompilerParams(
            collective_id=0, has_side_effects=True, vmem_limit_bytes=60 * 1024 * 1024
        ),
    )(
        tokens,
        norm_gain.reshape(1, D),
        w_query,
        w_key,
        w_decay,
        w_value,
        w_outgate,
        decay_rate.reshape(1, QC),
        state.reshape(S, QC, VC),
        head_gain.reshape(1, VC),
        w_output,
        moe_gain.reshape(1, D),
        expert_ids,
        group_prob.reshape(S, 1),
        inner_prob,
        w_gate.reshape(D, FB),
        w_up.reshape(D, FB),
        w_down.reshape(FB, D),
    )


def solution(mesh):
    placed = (
        P("ep", None),
        P(),
        P("ep", "tp"),
        P("ep", "tp"),
        P("ep", "tp"),
        P("ep", "tp"),
        P("ep", "tp"),
        P("tp"),
        P("ep", "tp", None, None),
        P(),
        P("tp", None),
        P(),
        P("ep", None),
        P("ep"),
        P("ep", None),
        P("ep", None, "tp"),
        P("ep", None, "tp"),
        P("ep", "tp", None),
    )
    return jax.shard_map(
        functools.partial(on_device, mesh.shape["ep"], mesh.shape["tp"]),
        mesh=mesh,
        in_specs=placed,
        out_specs=P("ep", "tp"),
        check_vma=False,
    )
```

time: 195 us -> 86.5 us (0.44)
  waiting for transfers between devices: 113 us -> 0 us
  Pallas kernels: 0 us -> 81 us
  blocking collectives: 31.8 us -> 0 us
  starting transfers between devices: 15.1 us -> 0 us
  between operations: 13.6 us -> 0.01 us
  matrix products: 11.2 us -> 0 us
  other arithmetic: 2.53 us -> 0 us
    pallas_call x0 -> x1, Pallas kernels: none -> 81 us  [on_device(): pl.pallas_call(functools.partial(kernel, E, T), out_shape=jax.ShapeDtypeS...]
    all_gather x1 -> x0, waiting for transfers between devices: 77.9 us -> none  [sent_together(): filled, at, done = (lax.all_gather(both, axis, axis=dim, tiled=True), 0, [])]
    all_to_all x3 -> x0, waiting for transfers between devices: 35.5 us -> none  [the longest x1 15.7 us: sent_to_all(): lax.all_to_all(jnp.broadcast_to(shard[None], (length, *shard.shape)), axi...]
    all_to_all x1 -> x0, blocking collectives: 31.8 us -> none  [on_device(): lax.all_to_all(sending, 'ep', split_axis=0, concat_axis=0, tiled=True)]
    all_to_all x3 -> x0, starting transfers between devices: 15.1 us -> none  [the longest x1 6.53 us: sent_to_all(): lax.all_to_all(jnp.broadcast_to(shard[None], (length, *shard.shape)), axi...]
    dot_general x10 -> x0, matrix products: 11.2 us -> none  [the longest x4 5.61 us: on_device(): jnp.dot(normed, piece, preferred_element_type=wide)]
    reduce_sum x8 -> x0, other arithmetic: 2.28 us -> none  [the longest x3 1.22 us: inverse_rms(): jnp.mean(values * values, axis=-1, keepdims=True) + epsilon]
    unnamed x29 -> x3, local copies, waits for them, and re-layouts: 3.91 us -> 3.97 us
  transfers between devices with their start and end apart: 4 -> 0, of which waited for: 4 -> 0; matrix products, arithmetic and copies ran while one was open for 1% -> 0% of each run, Pallas kernels for 0% -> 0%
where the time goes in v1:
time: 86.5 us; the launch traced here: 86.3 us
  Pallas kernels  81 us (94%)
  local copies, waits for them, and re-layouts  5.28 us (6%)
    pallas_call x1, Pallas kernels, on_device(): pl.pallas_call(functools.partial(kernel, E, T), out_shape=jax.ShapeDtypeS...  81 us
    unnamed x3, local copies, waits for them, and re-layouts  3.97 us

profile of v1, /device:TPU:1, one launch (start us, length us, event | category | flops | bytes accessed | tf_op | source)
XLA Modules:
  0.0 86.3 jit_solution(10631197681016784290)
XLA Ops:
  0.0 1.3 %copy.19.expert_ids = s32[16,2]{1,0:T(8,128)} copy(s32[16,2]{0,1:T(2,128)} %param.30) | data formatting | bytes 256 | tf_op args[12]
  1.3 1.3 %copy.20.group_prob = f32[16,1]{1,0:T(8,128)} copy(f32[16,1]{0,1:T(1,128)} %bitcast.17) | data formatting | bytes 128 | tf_op jit(solution)/shard_map/reshape | solution.py:467
  2.7 1.3 %copy.21.inner_prob = f32[16,2]{1,0:T(8,128)} copy(f32[16,2]{0,1:T(2,128)} %param.32) | data formatting | bytes 256 | tf_op args[14]
  4.0 81.0 %shard_map.172 = bf16[16,128]{1,0:T(8,128)(2,1)} custom-call(bf16[16,2048]{1,0:T(8,128)(2,1)} %tokens.1, f32[1,2048]{1,0:T(1,128)} %bitcast.13, bf16[64,128]{1,0:T(8,128)(2,1)} %w_query.1, bf16[64,128]{1,0:T(8,128)(2,1)} %w_key.1, bf16[64,128]{1,0:T(8,128)(2,1)} %w_decay.1, bf16[64,256]{1,0:T(8,128)(2,1)} %w_value.1, bf16[64,256]{1,0:T(8,128)(2,1)} %w_outgate.1, ...), custom_call_target="tpu_custom_call" | custom-call | tf_op jit(solution)/shard_map/pallas_call | solution.py:416
  85.0 1.3 %copy.23 = bf16[16,128]{1,0:T(8,128)(2,1)} copy(bf16[16,128]{1,0:T(8,128)(2,1)} %shard_map.172) | data formatting | bytes 8192
